TPU v7x, 32 devices: a whole 2x2x4 slice. The times are simulated.
32 devices in a mesh: sp: 8 (over z, y), tp: 4 (over x, core).
Axes of the slice: x: 2, y: 2, z: 4, core: 2. Of those that a mesh axis runs over, the one named last changes fastest.
Arguments:
- skip_stream: bfloat16 [6144, 2048], P(('sp', 'tp')), may hold values from -24 to 24
- acceptance_signal: bfloat16 [6144, 2048], P('sp', 'tp'), may hold values from -6 to 6
- lookup_mapped: bfloat16 [6144, 2048], P('sp', 'tp'), may hold values from -12 to 12
- payload_mapped: bfloat16 [6144, 2048], P('sp', 'tp'), may hold values from -6 to 6
- result_switch: bfloat16 [6144, 2048], P('sp', 'tp'), may hold values from -6 to 6
- forget_dynamic_share: bfloat16 [6144, 2048], P('sp', 'tp'), may hold values from -4 to 4
- additive_forget_logarithm: float32 [6144, 32], P('sp', 'tp'), may hold values from -1 to 0
- forget_feature_offset: float32 [2048], P('tp'), may hold values from -11 to -3
- substitution_dynamic_share: bfloat16 [6144, 2048], P('sp', 'tp'), may hold values from -6 to 6
- substitution_feature_offset: float32 [2048], P('tp'), may hold values from -6.5 to 2.5
- diagonal_reward_scales: float32 [2048], P('tp'), may hold values from -0.9 to 0.9
- result_matrix: bfloat16 [2048, 2048], P('tp'), may hold values from -0.125 to 0.125
- mlp_rescaler: float32 [2048], replicated, may hold values from 0.1 to 1.9
- switch_matrix: bfloat16 [2048, 5120], P('sp', 'tp'), may hold values from -0.125 to 0.125
- expand_matrix: bfloat16 [2048, 5120], P('sp', 'tp'), may hold values from -0.125 to 0.125
- contract_matrix: bfloat16 [2048, 5120], P('sp', 'tp'), may hold values from -0.25 to 0.25
Outputs:
- mixed_out: bfloat16 [6144, 2048], P(('sp', 'tp'))
All inputs are finite; a program needn't handle non-finite values.
Results may differ from a plain program's by a relative error of at most 0.015.
Values may be sent and summed in bfloat16 or wider, within the bound.
A program may use at most 128 MiB of HBM per device.

v0:
```python
import jax
import jax.numpy as jnp
from jax import lax
from jax.sharding import PartitionSpec as P

PER_GROUP_DIMS = 64


norm_eps = 1e-06
group_eps = 0.00064
half_step = 0.5
exact = lax.Precision.HIGHEST


def prefix(shard, axis, join, neutral):
    place = lax.axis_index(axis)
    gathered = jax.tree.map(
        lambda a, kind: lax.all_gather(a.astype(kind), axis), shard, (jnp.bfloat16, jnp.bfloat16)
    )
    state = jax.tree.map(lambda a, e: jnp.zeros_like(a) + jnp.asarray(e, a.dtype), shard, neutral)

    def one(turn, state):
        return join(
            state,
            jax.tree.map(
                lambda a, own: lax.dynamic_index_in_dim(a, turn, 0, False).astype(own.dtype),
                gathered,
                shard,
            ),
        )

    return lax.fori_loop(0, place, one, state)


def compose(earlier, latter):
    prod_first, carry_first = earlier
    prod_second, carry_second = latter
    product = jnp.einsum("hij,hjk->hik", prod_first, prod_second, precision=exact)
    carried = jnp.einsum("hij,hjk->hik", carry_first, prod_second, precision=exact) + carry_second
    return (product, carried)


def masked_pairs(left, right, keep):
    return jnp.where(keep, jnp.einsum("htc,hjc->htj", left, right, precision=exact), 0.0)


def block_step(carry, inputs):
    state_part, transition = carry
    read_blk, logstep_blk, key_blk, value_blk, unit_blk, rate_blk = inputs
    length = read_blk.shape[1]
    width = value_blk.shape[2]
    cumulate = jnp.cumsum(logstep_blk, axis=1)
    growth = jnp.exp(cumulate)
    shrink = jnp.exp(-cumulate)
    before_unit = jnp.exp(cumulate - logstep_blk) * unit_blk
    erase_dir = unit_blk * rate_blk
    key_back = key_blk * shrink
    erase_back = erase_dir * shrink
    read_fwd = read_blk * growth
    end_growth = growth[:, -1:, :]
    key_end = key_back * end_growth
    erase_end = erase_back * end_growth
    row_index = lax.broadcasted_iota(jnp.int32, (length, length), 0)
    col_index = lax.broadcasted_iota(jnp.int32, (length, length), 1)
    strict = col_index < row_index
    inclusive = col_index <= row_index
    key_past = masked_pairs(before_unit, key_back, strict)
    erase_past = masked_pairs(before_unit, erase_back, strict)
    key_read = masked_pairs(read_fwd, key_back, inclusive)
    erase_read = masked_pairs(read_fwd, erase_back, inclusive)
    recall_rhs = jnp.einsum("htk,hvk->htv", before_unit, state_part, precision=exact) + jnp.einsum(
        "htj,hjv->htv", key_past, value_blk, precision=exact
    )
    solved = jax.scipy.linalg.solve_triangular(
        erase_past,
        jnp.concatenate([recall_rhs, before_unit], axis=-1),
        lower=True,
        unit_diagonal=True,
    )
    recalled = solved[..., :width]
    carried_map = solved[..., width:]
    local_out = (
        jnp.einsum("htk,hvk->htv", read_fwd, state_part, precision=exact)
        + jnp.einsum("htj,hjv->htv", key_read, value_blk, precision=exact)
        - jnp.einsum("htj,hjv->htv", erase_read, recalled, precision=exact)
    )
    from_start = read_fwd - jnp.einsum("htj,hjk->htk", erase_read, carried_map, precision=exact)
    coefficient = jnp.einsum("htk,hjk->htj", from_start, transition, precision=exact)
    new_state = (
        state_part * end_growth
        + jnp.einsum("htv,htk->hvk", value_blk, key_end, precision=exact)
        - jnp.einsum("htv,htk->hvk", recalled, erase_end, precision=exact)
    )
    step_map = jnp.eye(width, dtype=jnp.float32)[None] * end_growth - jnp.einsum(
        "htj,htk->hjk", carried_map, erase_end, precision=exact
    )
    new_transition = jnp.einsum("hij,hjk->hik", transition, step_map, precision=exact)
    return ((new_state, new_transition), (local_out, coefficient))


def per_device(
    skip_stream,
    acceptance_signal,
    lookup_mapped,
    payload_mapped,
    result_switch,
    forget_dynamic_share,
    additive_forget_logarithm,
    forget_feature_offset,
    substitution_dynamic_share,
    substitution_feature_offset,
    diagonal_reward_scales,
    result_matrix,
    mlp_rescaler,
    switch_matrix,
    expand_matrix,
    contract_matrix,
):
    matrix_length, matrix_breadth = acceptance_signal.shape
    attention_groups = matrix_breadth // PER_GROUP_DIMS
    gate_whole, up_whole, down_whole = (
        lax.all_gather(switch_matrix, "sp", axis=0, tiled=True),
        lax.all_gather(expand_matrix, "sp", axis=0, tiled=True),
        lax.all_gather(contract_matrix, "sp", axis=0, tiled=True),
    )

    def by_head(values):
        return values.astype(jnp.float32).reshape(matrix_length, attention_groups, PER_GROUP_DIMS)

    acceptance_lines = by_head(acceptance_signal)
    lookup_vectors = by_head(lookup_mapped)
    payload_vectors = by_head(payload_mapped)
    log_decay_rate = (
        -jax.nn.softplus(
            -(forget_feature_offset[None, :] + forget_dynamic_share.astype(jnp.float32))
        )
        - 0.5
    )
    log_step = (
        -jnp.exp(log_decay_rate).reshape(matrix_length, attention_groups, PER_GROUP_DIMS)
        + additive_forget_logarithm[:, :, None]
    )
    replace_rate = jax.nn.sigmoid(
        substitution_feature_offset[None, :] + substitution_dynamic_share.astype(jnp.float32)
    )
    replace_rate = replace_rate.reshape(matrix_length, attention_groups, PER_GROUP_DIMS)
    unit_key = lookup_vectors * lax.rsqrt(
        jnp.sum(lookup_vectors * lookup_vectors, axis=-1, keepdims=True) + norm_eps
    )
    block_len = min(64, matrix_length)
    block_count = matrix_length // block_len

    def to_blocks(values):
        return values.reshape(block_count, block_len, attention_groups, PER_GROUP_DIMS).transpose(
            0, 2, 1, 3
        )

    def from_blocks(values):
        return values.transpose(0, 2, 1, 3).reshape(matrix_length, attention_groups, PER_GROUP_DIMS)

    identity_mats = jnp.broadcast_to(
        jnp.eye(PER_GROUP_DIMS, dtype=jnp.float32),
        (attention_groups, PER_GROUP_DIMS, PER_GROUP_DIMS),
    )
    zero_mats = jnp.zeros((attention_groups, PER_GROUP_DIMS, PER_GROUP_DIMS), jnp.float32)
    (closing_state, closing_map), (local_blocks, coef_blocks) = lax.scan(
        block_step,
        (zero_mats, identity_mats),
        (
            to_blocks(acceptance_lines),
            to_blocks(log_step),
            to_blocks(lookup_vectors),
            to_blocks(payload_vectors),
            to_blocks(unit_key),
            to_blocks(replace_rate),
        ),
    )
    _, carried = prefix((closing_map, closing_state), "sp", compose, (identity_mats, zero_mats))
    outcome = from_blocks(local_blocks) + jnp.einsum(
        "hvk,thk->thv", carried, from_blocks(coef_blocks), precision=exact
    )
    centre = jnp.mean(outcome, axis=-1, keepdims=True)
    spread = jnp.mean(jnp.square(outcome - centre), axis=-1, keepdims=True)
    rescaled_attention = (outcome - centre) * lax.rsqrt(spread + group_eps)
    diagonal_reward_summand = (
        jnp.sum(
            acceptance_lines
            * lookup_vectors
            * diagonal_reward_scales.reshape(attention_groups, PER_GROUP_DIMS),
            axis=-1,
            keepdims=True,
        )
        * payload_vectors
    )
    merged_attention = (
        (rescaled_attention + diagonal_reward_summand).reshape(matrix_length, matrix_breadth)
        * result_switch.astype(jnp.float32)
    ).astype(jnp.bfloat16)
    row_block = merged_attention
    projected = lax.psum_scatter(
        jnp.dot(row_block, result_matrix, preferred_element_type=jnp.float32).astype(jnp.bfloat16),
        "tp",
        scatter_dimension=0,
        tiled=True,
    )
    stream = skip_stream.astype(jnp.float32) + lax.optimization_barrier(projected).astype(
        jnp.float32
    )
    scale_rows = lax.rsqrt(jnp.mean(stream * stream, axis=-1, keepdims=True) + norm_eps)
    normed_rows = (stream * scale_rows * mlp_rescaler[None, :]).astype(jnp.bfloat16)
    whole_rows = lax.all_gather(normed_rows, "tp", axis=0, tiled=True)
    gate_act = jnp.dot(whole_rows, gate_whole, preferred_element_type=jnp.float32)
    up_act = jnp.dot(whole_rows, up_whole, preferred_element_type=jnp.float32)
    hidden = (jax.nn.silu(gate_act) * up_act).astype(jnp.bfloat16)
    row_block = hidden
    ffn_out = lax.psum_scatter(
        lax.dot_general(
            row_block, down_whole, (((1,), (1,)), ((), ())), preferred_element_type=jnp.float32
        ).astype(jnp.bfloat16),
        "tp",
        scatter_dimension=0,
        tiled=True,
    )
    return (stream + half_step * lax.optimization_barrier(ffn_out).astype(jnp.float32)).astype(
        jnp.bfloat16
    )


def solution(mesh):
    placed = (
        P(("sp", "tp"), None),
        P("sp", "tp"),
        P("sp", "tp"),
        P("sp", "tp"),
        P("sp", "tp"),
        P("sp", "tp"),
        P("sp", "tp"),
        P("tp"),
        P("sp", "tp"),
        P("tp"),
        P("tp"),
        P("tp", None),
        P(),
        P("sp", "tp"),
        P("sp", "tp"),
        P("sp", "tp"),
    )
    return jax.shard_map(
        per_device, mesh=mesh, in_specs=placed, out_specs=P(("sp", "tp"), None), check_vma=False
    )
```

profile of v0, /device:TPU:0, one launch (start us, length us, event | category | flops | bytes accessed | tf_op | source)
XLA Modules:
  0.0 1402.7 jit_solution(8593175602504717770)
XLA Ops:
  41.8 7.2 multiply_bitcast_fusion
  49.7 873.4 %while.30 = (s32[]{:T(128)}, f32[8,64,64]{2,1,0:T(8,128)}, f32[8,64,64]{1,2,0:T(8,128)}, f32[12,8,64,64]{3,2,1,0:T(8,128)}, f32[12,8,64,64]{3,2,1,0:T(8,128)}, /...) while((s32[]{:T(128)}, f32[8,64,64]{2,1,0:T(8,128)}, ...), condition=%wide.region_3.4_spmd.clone, body=%wide.region_1.3_spmd.clone.sunk | while | flops 431059008 | bytes 15468349 | solution.py:166
  51.5 6.3 fusion.174
  70.3 40.7 %custom-call.9 = f32[8,1,64,64]{2,3,1,0:T(8,128)} custom-call(f32[8,1,64,64]{3,2,1,0:T(8,128)} %fusion.178), custom_call_target="InvertDiagBlocksLowerTriangular" | custom-call | tf_op jit(solution)/shard_map/while/body/eval_jaxpr/jit(_solve_triangular)/vmap()/triangular_solve | solution.py:74
  122.5 6.3 fusion.174
  142.2 40.7 %custom-call.9 = f32[8,1,64,64]{2,3,1,0:T(8,128)} custom-call(f32[8,1,64,64]{3,2,1,0:T(8,128)} %fusion.178), custom_call_target="InvertDiagBlocksLowerTriangular" | custom-call | tf_op jit(solution)/shard_map/while/body/eval_jaxpr/jit(_solve_triangular)/vmap()/triangular_solve | solution.py:74
  195.4 6.3 fusion.174
  215.1 40.7 %custom-call.9 = f32[8,1,64,64]{2,3,1,0:T(8,128)} custom-call(f32[8,1,64,64]{3,2,1,0:T(8,128)} %fusion.178), custom_call_target="InvertDiagBlocksLowerTriangular" | custom-call | tf_op jit(solution)/shard_map/while/body/eval_jaxpr/jit(_solve_triangular)/vmap()/triangular_solve | solution.py:74
  268.4 6.3 fusion.174
  288.1 40.7 %custom-call.9 = f32[8,1,64,64]{2,3,1,0:T(8,128)} custom-call(f32[8,1,64,64]{3,2,1,0:T(8,128)} %fusion.178), custom_call_target="InvertDiagBlocksLowerTriangular" | custom-call | tf_op jit(solution)/shard_map/while/body/eval_jaxpr/jit(_solve_triangular)/vmap()/triangular_solve | solution.py:74
  341.3 6.3 fusion.174
  361.1 40.7 %custom-call.9 = f32[8,1,64,64]{2,3,1,0:T(8,128)} custom-call(f32[8,1,64,64]{3,2,1,0:T(8,128)} %fusion.178), custom_call_target="InvertDiagBlocksLowerTriangular" | custom-call | tf_op jit(solution)/shard_map/while/body/eval_jaxpr/jit(_solve_triangular)/vmap()/triangular_solve | solution.py:74
  414.3 6.3 fusion.174
  434.0 40.7 %custom-call.9 = f32[8,1,64,64]{2,3,1,0:T(8,128)} custom-call(f32[8,1,64,64]{3,2,1,0:T(8,128)} %fusion.178), custom_call_target="InvertDiagBlocksLowerTriangular" | custom-call | tf_op jit(solution)/shard_map/while/body/eval_jaxpr/jit(_solve_triangular)/vmap()/triangular_solve | solution.py:74
  487.2 6.3 fusion.174
  506.9 40.7 %custom-call.9 = f32[8,1,64,64]{2,3,1,0:T(8,128)} custom-call(f32[8,1,64,64]{3,2,1,0:T(8,128)} %fusion.178), custom_call_target="InvertDiagBlocksLowerTriangular" | custom-call | tf_op jit(solution)/shard_map/while/body/eval_jaxpr/jit(_solve_triangular)/vmap()/triangular_solve | solution.py:74
  579.8 40.7 %custom-call.9 = f32[8,1,64,64]{2,3,1,0:T(8,128)} custom-call(f32[8,1,64,64]{3,2,1,0:T(8,128)} %fusion.178), custom_call_target="InvertDiagBlocksLowerTriangular" | custom-call | tf_op jit(solution)/shard_map/while/body/eval_jaxpr/jit(_solve_triangular)/vmap()/triangular_solve | solution.py:74
  652.8 40.7 %custom-call.9 = f32[8,1,64,64]{2,3,1,0:T(8,128)} custom-call(f32[8,1,64,64]{3,2,1,0:T(8,128)} %fusion.178), custom_call_target="InvertDiagBlocksLowerTriangular" | custom-call | tf_op jit(solution)/shard_map/while/body/eval_jaxpr/jit(_solve_triangular)/vmap()/triangular_solve | solution.py:74
  725.7 40.7 %custom-call.9 = f32[8,1,64,64]{2,3,1,0:T(8,128)} custom-call(f32[8,1,64,64]{3,2,1,0:T(8,128)} %fusion.178), custom_call_target="InvertDiagBlocksLowerTriangular" | custom-call | tf_op jit(solution)/shard_map/while/body/eval_jaxpr/jit(_solve_triangular)/vmap()/triangular_solve | solution.py:74
  798.7 40.7 %custom-call.9 = f32[8,1,64,64]{2,3,1,0:T(8,128)} custom-call(f32[8,1,64,64]{3,2,1,0:T(8,128)} %fusion.178), custom_call_target="InvertDiagBlocksLowerTriangular" | custom-call | tf_op jit(solution)/shard_map/while/body/eval_jaxpr/jit(_solve_triangular)/vmap()/triangular_solve | solution.py:74
  851.9 6.3 fusion.174
  871.6 40.7 %custom-call.9 = f32[8,1,64,64]{2,3,1,0:T(8,128)} custom-call(f32[8,1,64,64]{3,2,1,0:T(8,128)} %fusion.178), custom_call_target="InvertDiagBlocksLowerTriangular" | custom-call | tf_op jit(solution)/shard_map/while/body/eval_jaxpr/jit(_solve_triangular)/vmap()/triangular_solve | solution.py:74
  924.2 36.5 %all-gather = bf16[64,64,64]{2,1,0:T(8,128)(2,1)} all-gather(bf16[8,64,64]{2,1,0:T(8,128)(2,1)S(1)} %copy.124), channel_id=2, replica_groups=mesh['sp'=8,'tp'=4] {'sp'}, dimensions={0}, use_global_device_ids=true | all-gather | bytes 589824 | tf_op jit(solution)/shard_map/all_gather | solution.py:18
  960.7 35.2 %all-gather.1 = bf16[64,64,64]{2,1,0:T(8,128)(2,1)} all-gather(bf16[8,64,64]{2,1,0:T(8,128)(2,1)S(1)} %convert_element_type.78), channel_id=3, replica_groups=mesh['sp'=8,'tp'=4] {'sp'}, dimensions={0}, use_global_device_ids=true | all-gather | bytes 589824 | tf_op jit(solution)/shard_map/all_gather | solution.py:18
  1033.1 54.8 %reduce-scatter.3.cloned.1.call-done = bf16[192,2048]{1,0:T(8,128)(2,1)} async-done(((bf16[768,2048]{1,0:T(8,128)(2,1)}), bf16[192,2048]{1,0:T(8,128)(2,1)}) %reduce-scatter.3.cloned.1.call-update) | async-done | bytes 786448 | tf_op jit(solution)/shard_map/reduce_scatter | solution.py:200
  1092.1 46.1 %all-gather.9.cloned.1.call-done = bf16[2048,1280]{1,0:T(8,128)(2,1)} async-done(((bf16[256,1280]{1,0:T(8,128)(2,1)}), bf16[2048,1280]{1,0:T(8,128)(2,1)}) %all-gather.9.cloned.1.call-update) | async-done | bytes 5242896 | tf_op jit(solution)/shard_map/all_gather | solution.py:122
  1138.2 28.1 %all-gather.7.cloned.1.call-done = bf16[768,2048]{1,0:T(8,128)(2,1)} async-done(((bf16[192,2048]{1,0:T(8,128)(2,1)}), bf16[768,2048]{1,0:T(8,128)(2,1)}) %all-gather.7.cloned.1.call-update) | async-done | bytes 3145744 | tf_op jit(solution)/shard_map/all_gather | solution.py:211
  1166.3 9.5 fusion.66
  1175.9 78.2 %all-gather.11.cloned.1.call-done = bf16[2048,1280]{1,0:T(8,128)(2,1)} async-done(((bf16[256,1280]{1,0:T(8,128)(2,1)}), bf16[2048,1280]{1,0:T(8,128)(2,1)}) %all-gather.11.cloned.1.call-update) | async-done | bytes 5242896 | tf_op jit(solution)/shard_map/all_gather | solution.py:123
  1254.1 86.1 %all-gather.13.cloned.1.call-done = bf16[2048,1280]{1,0:T(8,128)(2,1)} async-done(((bf16[256,1280]{1,0:T(8,128)(2,1)}), bf16[2048,1280]{1,0:T(8,128)(2,1)}) %all-gather.13.cloned.1.call-update) | async-done | bytes 5242896 | tf_op jit(solution)/shard_map/all_gather | solution.py:124
  1340.2 16.0 %convolution_convert_fusion.1 = bf16[768,2048]{1,0:T(8,128)(2,1)} fusion(bf16[2048,1280]{1,0:T(8,128)(2,1)} %all-gather.13.cloned.1.call-done, bf16[768,2048]{1,0:T(8,128)(2,1)} %all-gather.7.cloned.1.call-done, bf16[2048,1280]{1,0:T(8,128)(2,1)} %all-gather.11.cloned.1.call-done, f32[768,1280]{1,0:T(8,128)} %fusion.66), kind=kOutput, calls=%fused_computation.89 | convolution fusion | flops 8060534784 | bytes 20709376 | tf_op jit(solution)/shard_map/dot_general | solution.py:217
  1356.2 36.3 %reduce-scatter.5.cloned.1.call-done = bf16[192,2048]{1,0:T(8,128)(2,1)} async-done(((bf16[768,2048]{1,0:T(8,128)(2,1)}), bf16[192,2048]{1,0:T(8,128)(2,1)}) %reduce-scatter.5.cloned.1.call-update) | async-done | bytes 786448 | tf_op jit(solution)/shard_map/reduce_scatter | solution.py:216
  (564 shorter events, 413.2 us)
Async XLA Ops:
  7.4 1020.2 %copy-start = (bf16[512,2048]{1,0:T(8,128)(2,1)S(1)}, bf16[512,2048]{1,0:T(8,128)(2,1)}, u32[]{:S(2)}) copy-start(bf16[512,2048]{1,0:T(8,128)(2,1)} %param.31) | copy-start | bytes 6291460
  7.4 1080.6 %reduce-scatter.3.cloned.1.call-start = ((), (), s32[]{:S(2)}) async-start(), calls=%async_computation.2 | async-start | bytes 3932160 | tf_op jit(solution)/shard_map/reduce_scatter | solution.py:200
  18.0 3.3 copy-start.11
  22.7 3.6 copy-start.12
  22.7 3.6 copy-start.16
  28.7 3.4 copy-start.13
  32.3 3.4 copy-start.17
  113.4 3.1 copy-start.7
  116.0 2.9 copy-start.2
  186.4 3.1 copy-start.7
  259.3 3.1 copy-start.7
  261.9 2.9 copy-start.2
  332.3 3.1 copy-start.7
  405.2 3.1 copy-start.7
  478.1 3.1 copy-start.7
  551.1 3.1 copy-start.7
  624.0 3.1 copy-start.7
  697.0 3.1 copy-start.7
  769.9 3.1 copy-start.7
  772.5 2.9 copy-start.2
  842.9 3.1 copy-start.7
  915.8 3.1 copy-start.7
  918.4 2.9 copy-start.2
  923.1 37.6 %copy-start.3 = (f32[8,64,64]{2,1,0:T(8,128)S(1)}, f32[8,64,64]{2,1,0:T(8,128)}, u32[]{:S(2)}) copy-start(f32[8,64,64]{2,1,0:T(8,128)} %get-tuple-element.112) | copy-start | bytes 393220
  1024.4 3.1 copy-start.18
  1032.4 55.5 %copy-start.8 = (bf16[192,2048]{1,0:T(8,128)(2,1)S(1)}, bf16[192,2048]{1,0:T(8,128)(2,1)}, u32[]{:S(2)}) copy-start(bf16[192,2048]{1,0:T(8,128)(2,1)} %param.20) | copy-start | bytes 2359300
  1032.5 57.0 %copy-start.14 = (f32[2048]{0:T(1024)S(1)}, f32[2048]{0:T(1024)}, u32[]{:S(2)}) copy-start(f32[2048]{0:T(1024)} %param.32) | copy-start | bytes 24580
  1032.5 105.8 %all-gather.9.cloned.1.call-start = ((), (), s32[]{:S(2)}) async-start(), calls=%async_computation.4 | async-start | bytes 5898240 | tf_op jit(solution)/shard_map/all_gather | solution.py:122
  1033.0 133.3 %all-gather.7.cloned.1.call-start = ((), (), s32[]{:S(2)}) async-start(), calls=%async_computation.3 | async-start | bytes 3932160 | tf_op jit(solution)/shard_map/all_gather | solution.py:211
  1090.8 163.3 %all-gather.11.cloned.1.call-start = ((), (), s32[]{:S(2)}) async-start(), calls=%async_computation.5 | async-start | bytes 5898240 | tf_op jit(solution)/shard_map/all_gather | solution.py:123
  1091.3 248.8 %all-gather.13.cloned.1.call-start = ((), (), s32[]{:S(2)}) async-start(), calls=%async_computation.6 | async-start | bytes 5898240 | tf_op jit(solution)/shard_map/all_gather | solution.py:124
  1092.1 300.4 %reduce-scatter.5.cloned.1.call-start = ((), (), s32[]{:S(2)}) async-start(), calls=%async_computation.7 | async-start | bytes 3932160 | tf_op jit(solution)/shard_map/reduce_scatter | solution.py:216
  (59 other events, 151.8 us)
Sparse Core Ops, SparseCore 0:
  1032.6 55.3 reduce-scatter.2
  1356.3 36.1 reduce-scatter.4
Sparse Core Ops, SparseCore 1:
  1035.1 103.0 all-gather.8
  1139.7 26.6 all-gather.6
  1168.4 85.6 all-gather.10
  1256.3 83.9 all-gather.12
where the time goes:
time: 1410 us; the launch traced here: 1400 us
  other arithmetic  601 us (43%)
  waiting for transfers between devices  331 us (23%)
  matrix products  251 us (18%)
  local copies, waits for them, and re-layouts  131 us (9%)
  blocking collectives  71.7 us (5%)
  between operations  15.3 us (1%)
    another operation x36, other arithmetic, block_step(): jax.scipy.linalg.solve_triangular(erase_past, jnp.concatenate([recall_rhs...  488 us
    all_gather x1, waiting for transfers between devices, per_device(): lax.all_gather(contract_matrix, 'sp', axis=0, tiled=True)  86.1 us
    all_gather x1, waiting for transfers between devices, per_device(): lax.all_gather(expand_matrix, 'sp', axis=0, tiled=True)  78.2 us
    another operation x12, other arithmetic, block_step(): cumulate = jnp.cumsum(logstep_blk, axis=1)  75 us
    all_gather x2, blocking collectives, prefix(): lax.all_gather(a.astype(kind), axis)  71.7 us
    dynamic_slice x48, local copies, waits for them, and re-layouts, per_device(): lax.scan(block_step, (zero_mats, identity_mats), (to_blocks(acceptance_li...  68.7 us
    reduce_scatter x1, waiting for transfers between devices, per_device(): lax.psum_scatter(jnp.dot(row_block, result_matrix, preferred_element_type...  54.8 us
    dot_general x48, matrix products, masked_pairs(): jnp.einsum('htc,hjc->htj', left, right, precision=exact)  53.6 us
  transfers between devices with their start and end apart: 6, of which 6 were waited for; matrix products, arithmetic and copies ran while one was open for 1% of the time, Pallas kernels for 0%

commit v1 on v0

v1 whole, which is shorter than its diff:
```python
import functools

import jax
import jax.numpy as jnp
from jax import lax
from jax.experimental import pallas as pl
from jax.experimental.pallas import tpu as pltpu
from jax.sharding import PartitionSpec as P

PER_GROUP_DIMS = 64


norm_eps = 1e-06
group_eps = 0.00064
half_step = 0.5
exact = lax.Precision.HIGHEST

PAIR = 2 * PER_GROUP_DIMS
CHUNK = 64
ROWS_OUT = 256
NT = (((1,), (1,)), ((), ()))
NN = (((1,), (0,)), ((), ()))
TN = (((0,), (0,)), ((), ()))
bf16 = jnp.bfloat16
f32 = jnp.float32
P_SCORE, P_INV, P_SOLVE, P_OUT, P_STATE = 3, 1, 3, 3, 1


def mm(left, right, dims, passes):
    if passes == 6:
        return lax.dot_general(left, right, dims, precision=exact, preferred_element_type=f32)
    left_hi, right_hi = left.astype(bf16), right.astype(bf16)
    total = lax.dot_general(left_hi, right_hi, dims, preferred_element_type=f32)
    if passes == 3:
        left_lo = (left - left_hi.astype(f32)).astype(bf16)
        right_lo = (right - right_hi.astype(f32)).astype(bf16)
        total += lax.dot_general(left_hi, right_lo, dims, preferred_element_type=f32)
        total += lax.dot_general(left_lo, right_hi, dims, preferred_element_type=f32)
    return total


def halves(shape):
    return lax.broadcasted_iota(jnp.int32, shape, 1) < PER_GROUP_DIMS


def stack(values):
    first = halves(values.shape)
    zero = jnp.zeros_like(values)
    return jnp.concatenate([jnp.where(first, values, zero), jnp.where(first, zero, values)], 0)


def fold(values):
    size = values.shape[0] // 2
    return values[:size] + values[size:]


def head_sums(values):
    row = lax.broadcasted_iota(jnp.int32, (PAIR, PAIR), 0) // PER_GROUP_DIMS
    col = lax.broadcasted_iota(jnp.int32, (PAIR, PAIR), 1) // PER_GROUP_DIMS
    ones = jnp.where(row == col, 1.0, 0.0).astype(bf16)
    hi = values.astype(bf16)
    left = values - hi.astype(f32)
    mid = left.astype(bf16)
    low = (left - mid.astype(f32)).astype(bf16)
    return (
        jnp.dot(hi, ones, preferred_element_type=f32)
        + jnp.dot(mid, ones, preferred_element_type=f32)
        + jnp.dot(low, ones, preferred_element_type=f32)
    )


def recur_kernel(
    read_ref, key_ref, value_ref, forget_ref, added_ref, rate_ref, forget_off_ref, rate_off_ref,
    out_ref, coef_ref, state_out_ref, map_out_ref, memory,
):
    pairs = read_ref.shape[1] // PAIR
    span = range(pairs)
    row = lax.broadcasted_iota(jnp.int32, (PAIR, PAIR), 0)
    col = lax.broadcasted_iota(jnp.int32, (PAIR, PAIR), 1)
    diagonal = jnp.where(row == col, 1.0, 0.0)
    same_head = (row // CHUNK) == (col // CHUNK)
    strict = same_head & (col < row)
    inclusive = same_head & (col <= row)

    @pl.when(pl.program_id(0) == 0)
    def _():
        for p in span:
            memory[p, :PAIR] = jnp.zeros((PAIR, PAIR), f32)
            memory[p, PAIR:] = diagonal

    lower = (
        lax.broadcasted_iota(jnp.int32, (CHUNK, CHUNK), 1)
        <= lax.broadcasted_iota(jnp.int32, (CHUNK, CHUNK), 0)
    )
    lower = jnp.where(lower, 1.0, 0.0)
    first = halves((CHUNK, PAIR))
    at = [slice(p * PAIR, (p + 1) * PAIR) for p in span]
    decay_rate = [
        jax.nn.sigmoid(forget_off_ref[:, at[p]] + forget_ref[:, at[p]].astype(f32)) for p in span
    ]
    log_step = [
        -0.6065306597126334 * decay_rate[p]
        + jnp.where(first, added_ref[:, 2 * p : 2 * p + 1], added_ref[:, 2 * p + 1 : 2 * p + 2])
        for p in span
    ]
    cumulate = [mm(lower, log_step[p], NN, 6) for p in span]
    key = [key_ref[:, at[p]].astype(f32) for p in span]
    unit = [key[p] * lax.rsqrt(head_sums(key[p] * key[p]) + norm_eps) for p in span]
    erase = [
        unit[p] * jax.nn.sigmoid(rate_off_ref[:, at[p]] + rate_ref[:, at[p]].astype(f32))
        for p in span
    ]
    middle = [cumulate[p][CHUNK // 2 - 1 : CHUNK // 2] for p in span]
    last = [cumulate[p][CHUNK - 1 : CHUNK] for p in span]
    growth = [jnp.exp(cumulate[p] - middle[p]) for p in span]
    shrink = [jnp.exp(middle[p] - cumulate[p]) for p in span]
    to_middle = [jnp.exp(middle[p]) for p in span]
    from_middle = [jnp.exp(last[p] - middle[p]) for p in span]
    over_chunk = [jnp.exp(last[p]) for p in span]
    before = [jnp.exp(cumulate[p] - log_step[p] - middle[p]) * unit[p] for p in span]
    read = [read_ref[:, at[p]].astype(f32) * growth[p] for p in span]
    key_back = [key[p] * shrink[p] for p in span]
    erase_back = [erase[p] * shrink[p] for p in span]
    score = [
        mm(
            jnp.concatenate([stack(before[p]), stack(read[p])], 0),
            jnp.concatenate([stack(key_back[p]), stack(erase_back[p])], 0),
            NT,
            P_SCORE,
        )
        for p in span
    ]
    key_past = [jnp.where(strict, score[p][:PAIR, :PAIR], 0.0) for p in span]
    erase_past = [jnp.where(strict, score[p][:PAIR, PAIR:], 0.0) for p in span]
    key_read = [jnp.where(inclusive, score[p][PAIR:, :PAIR], 0.0) for p in span]
    erase_read = [jnp.where(inclusive, score[p][PAIR:, PAIR:], 0.0) for p in span]
    value = [stack(value_ref[:, at[p]]).astype(f32) for p in span]
    recall = [mm(key_past[p], value[p], NN, P_SOLVE) for p in span]
    inverse = [
        diagonal - jnp.where((row // 2) == (col // 2), erase_past[p], 0.0) for p in span
    ]
    size = 2
    while size < CHUNK:
        off = ((row // (2 * size)) == (col // (2 * size))) & ((row // size) != (col // size))
        part = [mm(jnp.where(off, erase_past[p], 0.0), inverse[p], NN, P_INV) for p in span]
        inverse = [inverse[p] - mm(inverse[p], part[p], NN, P_INV) for p in span]
        size *= 2
    solved = [
        mm(
            inverse[p],
            jnp.concatenate([recall[p], stack(before[p] * to_middle[p])], 1),
            NN,
            P_SOLVE,
        )
        for p in span
    ]
    inner = [
        mm(
            jnp.concatenate([key_read[p], -erase_read[p]], 1),
            jnp.concatenate(
                [jnp.concatenate([value[p], jnp.zeros_like(value[p])], 1), solved[p]], 0
            ),
            NN,
            P_OUT,
        )
        for p in span
    ]
    local = [fold(inner[p][:, :PAIR]) for p in span]
    from_start = [fold(inner[p][:, PAIR:]) + read[p] * to_middle[p] for p in span]
    both = [memory[p] for p in span]
    passed = [mm(from_start[p], both[p], NT, P_STATE) for p in span]
    for p in span:
        out_ref[:, at[p]] = local[p] + passed[p][:, :PAIR]
        coef_ref[:, at[p]] = passed[p][:, PAIR:].astype(bf16)
    key_end = [key_back[p] * from_middle[p] for p in span]
    erase_end = [erase_back[p] * from_middle[p] for p in span]
    recalled = [fold(solved[p][:, :PAIR]) for p in span]
    carried_map = [fold(solved[p][:, PAIR:]) for p in span]
    added = [
        mm(
            jnp.concatenate([value_ref[:, at[p]].astype(f32), -recalled[p]], 0),
            jnp.concatenate([key_end[p], erase_end[p]], 0),
            TN,
            P_OUT,
        )
        for p in span
    ]
    step_map = [mm(carried_map[p], erase_end[p], TN, P_OUT) for p in span]
    for p in span:
        moved = mm(both[p], jnp.where(same_head, step_map[p], 0.0), NN, P_STATE)
        kept = both[p] * over_chunk[p] - moved
        memory[p, :PAIR] = kept[:PAIR] + jnp.where(same_head, added[p], 0.0)
        memory[p, PAIR:] = kept[PAIR:]

    @pl.when(pl.program_id(0) == pl.num_programs(0) - 1)
    def _():
        for p in span:
            state_out_ref[p] = fold(memory[p, :PAIR]).astype(bf16)
            map_out_ref[p] = fold(memory[p, PAIR:]).astype(bf16)


def recurrence(read, key, value, forget, added, rate, forget_off, rate_off):
    length, breadth = read.shape
    pairs = breadth // PAIR
    wide = pl.BlockSpec((CHUNK, breadth), lambda c: (c, 0))
    vector = pl.BlockSpec((1, breadth), lambda c: (0, 0))
    closing = pl.BlockSpec((pairs, PER_GROUP_DIMS, PAIR), lambda c: (0, 0, 0))
    closing_shape = jax.ShapeDtypeStruct((pairs, PER_GROUP_DIMS, PAIR), bf16)
    return pl.pallas_call(
        recur_kernel,
        grid=(length // CHUNK,),
        in_specs=[
            wide, wide, wide, wide,
            pl.BlockSpec((CHUNK, added.shape[1]), lambda c: (c, 0)),
            wide, vector, vector,
        ],
        out_specs=[wide, wide, closing, closing],
        out_shape=[
            jax.ShapeDtypeStruct((length, breadth), f32),
            jax.ShapeDtypeStruct((length, breadth), bf16),
            closing_shape,
            closing_shape,
        ],
        scratch_shapes=[pltpu.VMEM((pairs, 2 * PAIR, PAIR), f32)],
        cost_estimate=pl.CostEstimate(
            flops=length * breadth * 200000, bytes_accessed=length * breadth * 16, transcendentals=0
        ),
        name="recurrence",
    )(read, key, value, forget, added, rate, forget_off[None, :], rate_off[None, :])


def merge_kernel(
    place_ref, local_ref, coef_ref, states_ref, maps_ref, read_ref, key_ref, value_ref,
    switch_ref, scales_ref, matrix_ref, out_ref, carried, merged,
):
    pairs = local_ref.shape[1] // PAIR
    span = range(pairs)

    @pl.when(pl.program_id(0) == 0)
    def _():
        for p in span:
            carried[p] = jnp.zeros((PAIR, PAIR), f32)

        def one(turn, _):
            for p in span:
                carried[p] = mm(
                    carried[p], stack(maps_ref[turn, p].astype(f32)), NN, 3
                ) + stack(states_ref[turn, p].astype(f32))
            return 0

        lax.fori_loop(0, place_ref[0], one, 0)

    for p in span:
        at = slice(p * PAIR, (p + 1) * PAIR)
        outcome = local_ref[:, at] + mm(coef_ref[:, at].astype(f32), carried[p], NT, 1)
        centred = outcome - head_sums(outcome) * (1.0 / PER_GROUP_DIMS)
        spread = head_sums(centred * centred) * (1.0 / PER_GROUP_DIMS)
        normed = centred * lax.rsqrt(spread + group_eps)
        reward = head_sums(
            read_ref[:, at].astype(f32) * key_ref[:, at].astype(f32) * scales_ref[:, at]
        )
        merged[:, at] = (
            (normed + reward * value_ref[:, at].astype(f32)) * switch_ref[:, at].astype(f32)
        ).astype(bf16)
    out_ref[...] = jnp.dot(merged[...], matrix_ref[...], preferred_element_type=f32).astype(bf16)


def merge(place, local, coef, states, maps, read, key, value, switch, scales, matrix):
    length, breadth = local.shape
    pairs = breadth // PAIR
    rows = ROWS_OUT if length % ROWS_OUT == 0 else CHUNK
    wide = pl.BlockSpec((rows, breadth), lambda c: (c, 0))
    whole = pl.BlockSpec(states.shape, lambda c: (0, 0, 0, 0))
    return pl.pallas_call(
        merge_kernel,
        grid=(length // rows,),
        in_specs=[
            pl.BlockSpec(memory_space=pltpu.SMEM),
            wide, wide, whole, whole, wide, wide, wide, wide,
            pl.BlockSpec((1, breadth), lambda c: (0, 0)),
            pl.BlockSpec(matrix.shape, lambda c: (0, 0)),
        ],
        out_specs=pl.BlockSpec((rows, matrix.shape[1]), lambda c: (c, 0)),
        out_shape=jax.ShapeDtypeStruct((length, matrix.shape[1]), bf16),
        scratch_shapes=[pltpu.VMEM((pairs, PAIR, PAIR), f32), pltpu.VMEM((rows, breadth), bf16)],
        cost_estimate=pl.CostEstimate(
            flops=2 * length * breadth * matrix.shape[1],
            bytes_accessed=length * breadth * 14 + 2 * matrix.size + 2 * length * matrix.shape[1],
            transcendentals=0,
        ),
        name="merge",
    )(place, local, coef, states, maps, read, key, value, switch, scales[None, :], matrix)


def per_device(
    skip_stream,
    acceptance_signal,
    lookup_mapped,
    payload_mapped,
    result_switch,
    forget_dynamic_share,
    additive_forget_logarithm,
    forget_feature_offset,
    substitution_dynamic_share,
    substitution_feature_offset,
    diagonal_reward_scales,
    result_matrix,
    mlp_rescaler,
    switch_matrix,
    expand_matrix,
    contract_matrix,
):
    gate_whole, up_whole, down_whole = (
        lax.all_gather(switch_matrix, "sp", axis=0, tiled=True),
        lax.all_gather(expand_matrix, "sp", axis=0, tiled=True),
        lax.all_gather(contract_matrix, "sp", axis=0, tiled=True),
    )
    local, coef, state, move = recurrence(
        acceptance_signal,
        lookup_mapped,
        payload_mapped,
        forget_dynamic_share,
        additive_forget_logarithm,
        substitution_dynamic_share,
        forget_feature_offset,
        substitution_feature_offset,
    )
    states = lax.all_gather(state, "sp")
    maps = lax.all_gather(move, "sp")
    partial_rows = merge(
        lax.axis_index("sp").astype(jnp.int32)[None],
        local,
        coef,
        states,
        maps,
        acceptance_signal,
        lookup_mapped,
        payload_mapped,
        result_switch,
        diagonal_reward_scales,
        result_matrix,
    )
    projected = lax.psum_scatter(
        partial_rows,
        "tp",
        scatter_dimension=0,
        tiled=True,
    )
    stream = skip_stream.astype(jnp.float32) + lax.optimization_barrier(projected).astype(
        jnp.float32
    )
    scale_rows = lax.rsqrt(jnp.mean(stream * stream, axis=-1, keepdims=True) + norm_eps)
    normed_rows = (stream * scale_rows * mlp_rescaler[None, :]).astype(jnp.bfloat16)
    whole_rows = lax.all_gather(normed_rows, "tp", axis=0, tiled=True)
    gate_act = jnp.dot(whole_rows, gate_whole, preferred_element_type=jnp.float32)
    up_act = jnp.dot(whole_rows, up_whole, preferred_element_type=jnp.float32)
    hidden = (jax.nn.silu(gate_act) * up_act).astype(jnp.bfloat16)
    row_block = hidden
    ffn_out = lax.psum_scatter(
        lax.dot_general(
            row_block, down_whole, (((1,), (1,)), ((), ())), preferred_element_type=jnp.float32
        ).astype(jnp.bfloat16),
        "tp",
        scatter_dimension=0,
        tiled=True,
    )
    return (stream + half_step * lax.optimization_barrier(ffn_out).astype(jnp.float32)).astype(
        jnp.bfloat16
    )


def solution(mesh):
    placed = (
        P(("sp", "tp"), None),
        P("sp", "tp"),
        P("sp", "tp"),
        P("sp", "tp"),
        P("sp", "tp"),
        P("sp", "tp"),
        P("sp", "tp"),
        P("tp"),
        P("sp", "tp"),
        P("tp"),
        P("tp"),
        P("tp", None),
        P(),
        P("sp", "tp"),
        P("sp", "tp"),
        P("sp", "tp"),
    )
    return jax.shard_map(
        per_device, mesh=mesh, in_specs=placed, out_specs=P(("sp", "tp"), None), check_vma=False
    )
```

time: 1410 us -> 491 us (0.35)
  other arithmetic: 601 us -> 6.21 us
  matrix products: 251 us -> 25.5 us
  local copies, waits for them, and re-layouts: 131 us -> 1.66 us
  Pallas kernels: 0 us -> 56.9 us
  waiting for transfers between devices: 331 us -> 316 us
    another operation x50 -> x0, other arithmetic: 563 us -> none  [the longest x36 488 us: block_step(): jax.scipy.linalg.solve_triangular(erase_past, jnp.concatenate([recall_rhs...]
    dot_general x182 -> x0, matrix products: 217 us -> none  [the longest x48 53.6 us: masked_pairs(): jnp.einsum('htc,hjc->htj', left, right, precision=exact)]
    dynamic_slice x48 -> x0, local copies, waits for them, and re-layouts: 68.7 us -> none  [per_device(): lax.scan(block_step, (zero_mats, identity_mats), (to_blocks(acceptance_li...]
    pallas_call x0 -> x2, Pallas kernels: none -> 56.9 us  [the longest x1 45.6 us: recurrence(): pl.pallas_call(recur_kernel, grid=(length // CHUNK,), in_specs=[wide, wid...]
    mul x14 -> x0, other arithmetic: 17.8 us -> none  [the longest x12 11.3 us: block_step(): erase_back = erase_dir * shrink]
    reduce_scatter x1, waiting for transfers between devices: 54.8 us -> 40.5 us  [per_device(): lax.psum_scatter(partial_rows, 'tp', scatter_dimension=0, tiled=True)]
  transfers between devices with their start and end apart: 6 -> 6, of which waited for: 6 -> 6; matrix products, arithmetic and copies ran while one was open for 1% -> 3% of each run, Pallas kernels for 0% -> 0%
where the time goes in v1:
time: 491 us
  waiting for transfers between devices  316 us (64%)
  blocking collectives  69.1 us (14%)
  Pallas kernels  56.9 us (12%)
  matrix products  25.5 us (5%)
  between operations  15.1 us (3%)
  other arithmetic  6.21 us (1%)
    all_gather x1, waiting for transfers between devices, per_device(): lax.all_gather(contract_matrix, 'sp', axis=0, tiled=True)  86.1 us
    all_gather x1, waiting for transfers between devices, per_device(): lax.all_gather(expand_matrix, 'sp', axis=0, tiled=True)  78.2 us
    pallas_call x1, Pallas kernels, recurrence(): pl.pallas_call(recur_kernel, grid=(length // CHUNK,), in_specs=[wide, wid...  45.6 us
    all_gather x1, waiting for transfers between devices, per_device(): lax.all_gather(switch_matrix, 'sp', axis=0, tiled=True)  44.9 us
    reduce_scatter x1, waiting for transfers between devices, per_device(): lax.psum_scatter(partial_rows, 'tp', scatter_dimension=0, tiled=True)  40.5 us
    reduce_scatter x1, waiting for transfers between devices, per_device(): lax.psum_scatter(lax.dot_general(row_block, down_whole, (((1,), (1,)), ((...  36.3 us
    all_gather x1, blocking collectives, per_device(): states = lax.all_gather(state, 'sp')  35.5 us
    all_gather x1, blocking collectives, per_device(): maps = lax.all_gather(move, 'sp')  33.6 us
  transfers between devices with their start and end apart: 6, of which 6 were waited for; matrix products, arithmetic and copies ran while one was open for 3% of the time, Pallas kernels for 0%

profile of v1, /device:TPU:0, one launch (start us, length us, event | category | flops | bytes accessed | tf_op | source)
XLA Modules:
  0.0 490.8 jit_solution(4885889694382055252)
XLA Ops:
  7.4 0.0 reduce-scatter.3.cloned.1.call-start
  7.4 1.6 copy.18.added_ref
  9.0 45.6 %recurrence.1 = (f32[768,512]{1,0:T(8,128)}, bf16[768,512]{1,0:T(8,128)(2,1)}, bf16[4,64,128]{2,1,0:T(8,128)(2,1)}, bf16[4,64,128]{2,1,0:T(8,128)(2,1)}) custom-call(bf16[768,512]{1,0:T(8,128)(2,1)} %read_ref.3, bf16[768,512]{1,0:T(8,128)(2,1)} %key_ref.3, bf16[768,512]{1,0:T(8,128)(2,1)} %value_ref.3, bf16[768,512]{1,0:T(8,128)(2,1)} %forget_ref.1, ...), custom_call_target="tpu_custom_call" | custom-call | flops 78643200000 | bytes 6291456 | tf_op jit(solution)/shard_map/recurrence/pallas_call | solution.py:209
  54.7 35.5 %all-gather = bf16[32,64,128]{2,1,0:T(8,128)(2,1)} all-gather(bf16[4,64,128]{2,1,0:T(8,128)(2,1)} %get-tuple-element.11), channel_id=2, replica_groups=mesh['sp'=8,'tp'=4] {'sp'}, dimensions={0}, use_global_device_ids=true | all-gather | bytes 589824 | tf_op jit(solution)/shard_map/all_gather | solution.py:328
  90.2 33.6 %all-gather.1 = bf16[32,64,128]{2,1,0:T(8,128)(2,1)} all-gather(bf16[4,64,128]{2,1,0:T(8,128)(2,1)} %get-tuple-element.12), channel_id=3, replica_groups=mesh['sp'=8,'tp'=4] {'sp'}, dimensions={0}, use_global_device_ids=true | all-gather | bytes 589824 | tf_op jit(solution)/shard_map/all_gather | solution.py:329
  123.8 11.3 %merge.1 = bf16[768,2048]{1,0:T(8,128)(2,1)} custom-call(s32[1]{0:T(128)} %bitcast.place_ref, f32[768,512]{1,0:T(8,128)} %get-tuple-element.9.local_ref, bf16[768,512]{1,0:T(8,128)(2,1)} %get-tuple-element.10.coef_ref, bf16[8,4,64,128]{3,2,1,0:T(8,128)(2,1)} %bitcast.11, bf16[8,4,64,128]{3,2,1,0:T(8,128)(2,1)} %bitcast.12, bf16[768,512]{1,0:T(8,128)(2,1)} %read_ref.3, ...), custom_call_target="tpu_custom_call" | custom-call | flops 1610612736 | bytes 10747904 | tf_op jit(solution)/shard_map/merge/pallas_call | solution.py:274
  135.1 0.0 copy-start.2
  135.1 0.0 reduce-scatter.3.cloned.1.call-update
  135.1 0.0 all-gather.9.cloned.1.call-start
  135.2 0.5 all-gather.9.cloned.1.call-update
  135.7 0.0 all-gather.7.cloned.1.call-start
  135.8 40.5 %reduce-scatter.3.cloned.1.call-done = bf16[192,2048]{1,0:T(8,128)(2,1)} async-done(((bf16[768,2048]{1,0:T(8,128)(2,1)}), bf16[192,2048]{1,0:T(8,128)(2,1)}) %reduce-scatter.3.cloned.1.call-update) | async-done | bytes 786448 | tf_op jit(solution)/shard_map/reduce_scatter | solution.py:343
  176.3 0.0 copy-done
  176.3 1.5 multiply_reduce_fusion
  177.7 0.0 copy-done.2
  177.7 2.3 multiply_convert_fusion
  180.1 0.0 all-gather.7.cloned.1.call-update
  180.1 0.0 all-gather.11.cloned.1.call-start
  180.1 0.5 all-gather.11.cloned.1.call-update
  180.7 0.0 all-gather.13.cloned.1.call-start
  180.7 0.7 all-gather.13.cloned.1.call-update
  181.4 0.2 reduce-scatter.5.cloned.1.call-start
  181.6 44.9 %all-gather.9.cloned.1.call-done = bf16[2048,1280]{1,0:T(8,128)(2,1)} async-done(((bf16[256,1280]{1,0:T(8,128)(2,1)}), bf16[2048,1280]{1,0:T(8,128)(2,1)}) %all-gather.9.cloned.1.call-update) | async-done | bytes 5242896 | tf_op jit(solution)/shard_map/all_gather | solution.py:314
  226.5 28.1 %all-gather.7.cloned.1.call-done = bf16[768,2048]{1,0:T(8,128)(2,1)} async-done(((bf16[192,2048]{1,0:T(8,128)(2,1)}), bf16[768,2048]{1,0:T(8,128)(2,1)}) %all-gather.7.cloned.1.call-update) | async-done | bytes 3145744 | tf_op jit(solution)/shard_map/all_gather | solution.py:354
  254.6 9.6 %fusion.2 = f32[768,1280]{1,0:T(8,128)} fusion(bf16[768,2048]{1,0:T(8,128)(2,1)} %all-gather.7.cloned.1.call-done, bf16[2048,1280]{1,0:T(8,128)(2,1)} %all-gather.9.cloned.1.call-done), kind=kOutput, calls=%fused_computation.9 | convolution fusion | flops 4026531840 | bytes 12320768 | tf_op jit(solution)/shard_map/dot_general | solution.py:355
  264.2 78.2 %all-gather.11.cloned.1.call-done = bf16[2048,1280]{1,0:T(8,128)(2,1)} async-done(((bf16[256,1280]{1,0:T(8,128)(2,1)}), bf16[2048,1280]{1,0:T(8,128)(2,1)}) %all-gather.11.cloned.1.call-update) | async-done | bytes 5242896 | tf_op jit(solution)/shard_map/all_gather | solution.py:315
  342.4 86.1 %all-gather.13.cloned.1.call-done = bf16[2048,1280]{1,0:T(8,128)(2,1)} async-done(((bf16[256,1280]{1,0:T(8,128)(2,1)}), bf16[2048,1280]{1,0:T(8,128)(2,1)}) %all-gather.13.cloned.1.call-update) | async-done | bytes 5242896 | tf_op jit(solution)/shard_map/all_gather | solution.py:316
  428.5 16.0 %convolution_convert_fusion = bf16[768,2048]{1,0:T(8,128)(2,1)} fusion(bf16[2048,1280]{1,0:T(8,128)(2,1)} %all-gather.13.cloned.1.call-done, bf16[768,2048]{1,0:T(8,128)(2,1)} %all-gather.7.cloned.1.call-done, bf16[2048,1280]{1,0:T(8,128)(2,1)} %all-gather.11.cloned.1.call-done, f32[768,1280]{1,0:T(8,128)} %fusion.2), kind=kOutput, calls=%fused_computation.2 | convolution fusion | flops 8060534784 | bytes 20709376 | tf_op jit(solution)/shard_map/dot_general | solution.py:360
  444.4 0.0 reduce-scatter.5.cloned.1.call-update
  444.5 36.3 %reduce-scatter.5.cloned.1.call-done = bf16[192,2048]{1,0:T(8,128)(2,1)} async-done(((bf16[768,2048]{1,0:T(8,128)(2,1)}), bf16[192,2048]{1,0:T(8,128)(2,1)}) %reduce-scatter.5.cloned.1.call-update) | async-done | bytes 786448 | tf_op jit(solution)/shard_map/reduce_scatter | solution.py:359
  480.7 0.0 copy-done.1
  480.7 2.4 add_convert_fusion
  (3 shorter events, 0.0 us)
Async XLA Ops:
  7.4 168.9 %reduce-scatter.3.cloned.1.call-start = ((), (), s32[]{:S(2)}) async-start(), calls=%async_computation.2 | async-start | bytes 3932160 | tf_op jit(solution)/shard_map/reduce_scatter | solution.py:343
  135.1 41.2 %copy-start = (bf16[192,2048]{1,0:T(8,128)(2,1)S(1)}, bf16[192,2048]{1,0:T(8,128)(2,1)}, u32[]{:S(2)}) copy-start(bf16[192,2048]{1,0:T(8,128)(2,1)} %param.16) | copy-start | bytes 2359300
  135.1 42.6 %copy-start.2 = (f32[2048]{0:T(1024)S(1)}, f32[2048]{0:T(1024)}, u32[]{:S(2)}) copy-start(f32[2048]{0:T(1024)} %param.28) | copy-start | bytes 24580
  135.1 91.4 %all-gather.9.cloned.1.call-start = ((), (), s32[]{:S(2)}) async-start(), calls=%async_computation.4 | async-start | bytes 5898240 | tf_op jit(solution)/shard_map/all_gather | solution.py:314
  135.7 118.9 %all-gather.7.cloned.1.call-start = ((), (), s32[]{:S(2)}) async-start(), calls=%async_computation.3 | async-start | bytes 3932160 | tf_op jit(solution)/shard_map/all_gather | solution.py:354
  180.1 162.3 %all-gather.11.cloned.1.call-start = ((), (), s32[]{:S(2)}) async-start(), calls=%async_computation.5 | async-start | bytes 5898240 | tf_op jit(solution)/shard_map/all_gather | solution.py:315
  180.7 247.8 %all-gather.13.cloned.1.call-start = ((), (), s32[]{:S(2)}) async-start(), calls=%async_computation.6 | async-start | bytes 5898240 | tf_op jit(solution)/shard_map/all_gather | solution.py:316
  181.4 299.3 %reduce-scatter.5.cloned.1.call-start = ((), (), s32[]{:S(2)}) async-start(), calls=%async_computation.7 | async-start | bytes 3932160 | tf_op jit(solution)/shard_map/reduce_scatter | solution.py:359
  444.4 36.3 %copy-start.1 = (bf16[192,2048]{1,0:T(8,128)(2,1)S(1)}, bf16[192,2048]{1,0:T(8,128)(2,1)}, u32[]{:S(2)}) copy-start(bf16[192,2048]{1,0:T(8,128)(2,1)} %reduce-scatter.3.cloned.1.call-done) | copy-start | bytes 2359300
Sparse Core Ops, SparseCore 0:
  135.3 40.9 reduce-scatter.2
  444.6 36.1 reduce-scatter.4
Sparse Core Ops, SparseCore 1:
  137.8 88.7 all-gather.8
  228.0 26.6 all-gather.6
  256.7 85.6 all-gather.10
  344.6 83.9 all-gather.12

commit v2 on v1

--- a/solution.py
+++ b/solution.py
@@ -229,6 +229,56 @@
     )(read, key, value, forget, added, rate, forget_off[None, :], rate_off[None, :])
 
 
+def share_kernel(mine_ref, all_ref, own_sem, send_sem, recv_sem):
+    me, n = lax.axis_index("sp"), all_ref.shape[0]
+    barrier = pltpu.get_barrier_semaphore()
+    for step in range(1, n):
+        pl.semaphore_signal(
+            barrier,
+            inc=1,
+            device_id={"sp": lax.rem(me + step, n)},
+            device_id_type=pl.DeviceIdType.MESH,
+        )
+    pl.semaphore_wait(barrier, n - 1)
+    copies = [
+        pltpu.make_async_remote_copy(
+            src_ref=mine_ref,
+            dst_ref=all_ref.at[me],
+            send_sem=send_sem.at[step - 1],
+            recv_sem=recv_sem.at[step - 1],
+            device_id={"sp": lax.rem(me + step, n)},
+            device_id_type=pl.DeviceIdType.MESH,
+        )
+        for step in range(1, n)
+    ]
+    for copy in copies:
+        copy.start()
+    own = pltpu.make_async_copy(mine_ref, all_ref.at[me], own_sem)
+    own.start()
+    own.wait()
+    for copy in copies:
+        copy.wait()
+
+
+def share(mine):
+    n = lax.axis_size("sp")
+    everyone = pl.pallas_call(
+        share_kernel,
+        in_specs=[pl.BlockSpec(memory_space=pltpu.VMEM)],
+        out_specs=pl.BlockSpec(memory_space=pltpu.VMEM),
+        out_shape=jax.ShapeDtypeStruct((n,) + mine.shape, mine.dtype),
+        scratch_shapes=[
+            pltpu.SemaphoreType.DMA,
+            pltpu.SemaphoreType.DMA((n - 1,)),
+            pltpu.SemaphoreType.DMA((n - 1,)),
+        ],
+        compiler_params=pltpu.CompilerParams(collective_id=0, has_side_effects=True),
+        cost_estimate=pl.CostEstimate(flops=0, bytes_accessed=40000000, transcendentals=0),
+        name="share",
+    )(mine)
+    return everyone[:, 0], everyone[:, 1]
+
+
 def merge_kernel(
     place_ref, local_ref, coef_ref, states_ref, maps_ref, read_ref, key_ref, value_ref,
     switch_ref, scales_ref, matrix_ref, out_ref, carried, merged,
@@ -325,8 +375,8 @@
         forget_feature_offset,
         substitution_feature_offset,
     )
-    states = lax.all_gather(state, "sp")
-    maps = lax.all_gather(move, "sp")
+    states, maps = share(jnp.stack([state, move]))
+    local, gate_whole = lax.optimization_barrier((local, gate_whole))
     partial_rows = merge(
         lax.axis_index("sp").astype(jnp.int32)[None],
         local,
@@ -351,6 +401,7 @@
     )
     scale_rows = lax.rsqrt(jnp.mean(stream * stream, axis=-1, keepdims=True) + norm_eps)
     normed_rows = (stream * scale_rows * mlp_rescaler[None, :]).astype(jnp.bfloat16)
+    normed_rows, up_whole = lax.optimization_barrier((normed_rows, up_whole))
     whole_rows = lax.all_gather(normed_rows, "tp", axis=0, tiled=True)
     gate_act = jnp.dot(whole_rows, gate_whole, preferred_element_type=jnp.float32)
     up_act = jnp.dot(whole_rows, up_whole, preferred_element_type=jnp.float32)

time: 491 us -> 435 us (0.89)
  blocking collectives: 69.1 us -> 0 us
  Pallas kernels: 56.9 us -> 99.5 us
  waiting for transfers between devices: 316 us -> 284 us
    all_gather x2 -> x0, blocking collectives: 69.1 us -> none  [the longest x1 35.5 us: per_device(): states = lax.all_gather(state, 'sp')]
    pallas_call x0 -> x1, Pallas kernels: none -> 42.5 us  [share(): pl.pallas_call(share_kernel, in_specs=[pl.BlockSpec(memory_space=pltpu.VM...]
    all_gather x1, waiting for transfers between devices: 44.9 us -> 17.5 us  [per_device(): lax.all_gather(switch_matrix, 'sp', axis=0, tiled=True)]
    all_gather x1, waiting for transfers between devices: 86.1 us -> 78.4 us  [per_device(): lax.all_gather(contract_matrix, 'sp', axis=0, tiled=True)]
    all_gather x1, waiting for transfers between devices: 78.2 us -> 84.3 us  [per_device(): lax.all_gather(expand_matrix, 'sp', axis=0, tiled=True)]
  transfers between devices with their start and end apart: 6 -> 6, of which waited for: 6 -> 6; matrix products, arithmetic and copies ran while one was open for 3% -> 4% of each run, Pallas kernels for 0% -> 20%
where the time goes in v2:
time: 435 us
  waiting for transfers between devices  284 us (65%)
  Pallas kernels  99.5 us (23%)
  matrix products  25.5 us (6%)
  between operations  13.5 us (3%)
  other arithmetic  7.74 us (2%)
    all_gather x1, waiting for transfers between devices, per_device(): lax.all_gather(expand_matrix, 'sp', axis=0, tiled=True)  84.3 us
    all_gather x1, waiting for transfers between devices, per_device(): lax.all_gather(contract_matrix, 'sp', axis=0, tiled=True)  78.4 us
    pallas_call x1, Pallas kernels, recurrence(): pl.pallas_call(recur_kernel, grid=(length // CHUNK,), in_specs=[wide, wid...  45.7 us
    pallas_call x1, Pallas kernels, share(): pl.pallas_call(share_kernel, in_specs=[pl.BlockSpec(memory_space=pltpu.VM...  42.5 us
    reduce_scatter x1, waiting for transfers between devices, per_device(): lax.psum_scatter(partial_rows, 'tp', scatter_dimension=0, tiled=True)  38.2 us
    reduce_scatter x1, waiting for transfers between devices, per_device(): lax.psum_scatter(lax.dot_general(row_block, down_whole, (((1,), (1,)), ((...  36.2 us
    all_gather x1, waiting for transfers between devices, per_device(): whole_rows = lax.all_gather(normed_rows, 'tp', axis=0, tiled=True)  27.3 us
    all_gather x1, waiting for transfers between devices, per_device(): lax.all_gather(switch_matrix, 'sp', axis=0, tiled=True)  17.5 us
  transfers between devices with their start and end apart: 6, of which 6 were waited for; matrix products, arithmetic and copies ran while one was open for 4% of the time, Pallas kernels for 20%

profile of v2, /device:TPU:0, one launch (start us, length us, event | category | flops | bytes accessed | tf_op | source)
XLA Modules:
  0.0 434.5 jit_solution(16075991706849202710)
XLA Ops:
  6.5 0.0 all-gather.5.cloned.1.call-start
  6.5 0.7 all-gather.5.cloned.1.call-update
  7.3 0.0 reduce-scatter.3.cloned.1.call-start
  7.3 1.7 copy.17.added_ref
  9.0 45.7 %recurrence.1 = (f32[768,512]{1,0:T(8,128)}, bf16[768,512]{1,0:T(8,128)(2,1)}, bf16[4,64,128]{2,1,0:T(8,128)(2,1)}, bf16[4,64,128]{2,1,0:T(8,128)(2,1)}) custom-call(bf16[768,512]{1,0:T(8,128)(2,1)} %read_ref.3, bf16[768,512]{1,0:T(8,128)(2,1)} %key_ref.3, bf16[768,512]{1,0:T(8,128)(2,1)} %value_ref.3, bf16[768,512]{1,0:T(8,128)(2,1)} %forget_ref.1, ...), custom_call_target="tpu_custom_call" | custom-call | flops 78643200000 | bytes 6291456 | tf_op jit(solution)/shard_map/recurrence/pallas_call | solution.py:209
  54.7 1.5 pad_maximum_fusion.mine_ref
  56.2 42.5 %share.1 = bf16[8,2,4,64,128]{4,3,2,1,0:T(8,128)(2,1)} custom-call(bf16[2,4,64,128]{3,2,1,0:T(8,128)(2,1)} %pad_maximum_fusion.mine_ref), custom_call_target="tpu_custom_call" | custom-call | bytes 40000000 | tf_op jit(solution)/shard_map/share/pallas_call | solution.py:265
  98.7 2.4 slice_bitcast_fusion
  101.0 17.5 %all-gather.5.cloned.1.call-done = bf16[2048,1280]{1,0:T(8,128)(2,1)} async-done(((bf16[256,1280]{1,0:T(8,128)(2,1)}), bf16[2048,1280]{1,0:T(8,128)(2,1)}) %all-gather.5.cloned.1.call-update) | async-done | bytes 5242896 | tf_op jit(solution)/shard_map/all_gather | solution.py:364
  118.5 11.3 %merge.1 = bf16[768,2048]{1,0:T(8,128)(2,1)} custom-call(s32[1]{0:T(128)} %bitcast.place_ref, f32[768,512]{1,0:T(8,128)} %get-tuple-element.14.local_ref, bf16[768,512]{1,0:T(8,128)(2,1)} %get-tuple-element.15.coef_ref, bf16[8,4,64,128]{3,2,1,0:T(8,128)(2,1)} %get-tuple-element.22.states_ref, bf16[8,4,64,128]{3,2,1,0:T(8,128)(2,1)} %get-tuple-element.21.maps_ref, ...), custom_call_target="tpu_custom_call" | custom-call | flops 1610612736 | bytes 10747904 | tf_op jit(solution)/shard_map/merge/pallas_call | solution.py:324
  129.8 0.0 copy-start.2
  129.8 0.0 reduce-scatter.3.cloned.1.call-update
  129.9 0.0 all-gather.7.cloned.1.call-start
  129.9 0.7 all-gather.7.cloned.1.call-update
  130.6 0.0 all-gather.9.cloned.1.call-start
  130.6 38.2 %reduce-scatter.3.cloned.1.call-done = bf16[192,2048]{1,0:T(8,128)(2,1)} async-done(((bf16[768,2048]{1,0:T(8,128)(2,1)}), bf16[192,2048]{1,0:T(8,128)(2,1)}) %reduce-scatter.3.cloned.1.call-update) | async-done | bytes 786448 | tf_op jit(solution)/shard_map/reduce_scatter | solution.py:393
  168.8 0.0 copy-done
  168.8 1.5 multiply_reduce_fusion
  170.3 2.3 multiply_convert_fusion
  172.6 84.3 %all-gather.7.cloned.1.call-done = bf16[2048,1280]{1,0:T(8,128)(2,1)} async-done(((bf16[256,1280]{1,0:T(8,128)(2,1)}), bf16[2048,1280]{1,0:T(8,128)(2,1)}) %all-gather.7.cloned.1.call-update) | async-done | bytes 5242896 | tf_op jit(solution)/shard_map/all_gather | solution.py:365
  257.0 0.0 all-gather.9.cloned.1.call-update
  257.0 0.0 all-gather.11.cloned.1.call-start
  257.0 0.5 all-gather.11.cloned.1.call-update
  257.6 0.2 reduce-scatter.5.cloned.1.call-start
  257.8 27.3 %all-gather.9.cloned.1.call-done = bf16[768,2048]{1,0:T(8,128)(2,1)} async-done(((bf16[192,2048]{1,0:T(8,128)(2,1)}), bf16[768,2048]{1,0:T(8,128)(2,1)}) %all-gather.9.cloned.1.call-update) | async-done | bytes 3145744 | tf_op jit(solution)/shard_map/all_gather | solution.py:405
  285.1 9.6 %fusion.2 = f32[768,1280]{1,0:T(8,128)} fusion(bf16[768,2048]{1,0:T(8,128)(2,1)} %all-gather.9.cloned.1.call-done, bf16[2048,1280]{1,0:T(8,128)(2,1)} %all-gather.5.cloned.1.call-done), kind=kOutput, calls=%fused_computation.12 | convolution fusion | flops 4026531840 | bytes 12320768 | tf_op jit(solution)/shard_map/dot_general | solution.py:406
  294.7 78.4 %all-gather.11.cloned.1.call-done = bf16[2048,1280]{1,0:T(8,128)(2,1)} async-done(((bf16[256,1280]{1,0:T(8,128)(2,1)}), bf16[2048,1280]{1,0:T(8,128)(2,1)}) %all-gather.11.cloned.1.call-update) | async-done | bytes 5242896 | tf_op jit(solution)/shard_map/all_gather | solution.py:366
  373.1 16.0 %convolution_convert_fusion = bf16[768,2048]{1,0:T(8,128)(2,1)} fusion(bf16[2048,1280]{1,0:T(8,128)(2,1)} %all-gather.11.cloned.1.call-done, bf16[768,2048]{1,0:T(8,128)(2,1)} %all-gather.9.cloned.1.call-done, bf16[2048,1280]{1,0:T(8,128)(2,1)} %all-gather.7.cloned.1.call-done, f32[768,1280]{1,0:T(8,128)} %fusion.2), kind=kOutput, calls=%fused_computation.2 | convolution fusion | flops 8060534784 | bytes 20709376 | tf_op jit(solution)/shard_map/dot_general | solution.py:411
  389.0 0.0 reduce-scatter.5.cloned.1.call-update
  389.0 36.2 %reduce-scatter.5.cloned.1.call-done = bf16[192,2048]{1,0:T(8,128)(2,1)} async-done(((bf16[768,2048]{1,0:T(8,128)(2,1)}), bf16[192,2048]{1,0:T(8,128)(2,1)}) %reduce-scatter.5.cloned.1.call-update) | async-done | bytes 786448 | tf_op jit(solution)/shard_map/reduce_scatter | solution.py:410
  425.3 0.0 copy-done.1
  425.3 2.4 add_convert_fusion
  (4 shorter events, 0.0 us)
Async XLA Ops:
  6.5 112.0 %all-gather.5.cloned.1.call-start = ((), (), s32[]{:S(2)}) async-start(), calls=%async_computation.2 | async-start | bytes 5898240 | tf_op jit(solution)/shard_map/all_gather | solution.py:364
  7.3 161.6 %reduce-scatter.3.cloned.1.call-start = ((), (), s32[]{:S(2)}) async-start(), calls=%async_computation.3 | async-start | bytes 3932160 | tf_op jit(solution)/shard_map/reduce_scatter | solution.py:393
  129.8 39.0 %copy-start = (bf16[192,2048]{1,0:T(8,128)(2,1)S(1)}, bf16[192,2048]{1,0:T(8,128)(2,1)}, u32[]{:S(2)}) copy-start(bf16[192,2048]{1,0:T(8,128)(2,1)} %param.16) | copy-start | bytes 2359300
  129.8 40.5 %copy-start.2 = (f32[2048]{0:T(1024)S(1)}, f32[2048]{0:T(1024)}, u32[]{:S(2)}) copy-start(f32[2048]{0:T(1024)} %param.28) | copy-start | bytes 24580
  129.9 127.1 %all-gather.7.cloned.1.call-start = ((), (), s32[]{:S(2)}) async-start(), calls=%async_computation.4 | async-start | bytes 5898240 | tf_op jit(solution)/shard_map/all_gather | solution.py:365
  130.6 154.5 %all-gather.9.cloned.1.call-start = ((), (), s32[]{:S(2)}) async-start(), calls=%async_computation.5 | async-start | bytes 3932160 | tf_op jit(solution)/shard_map/all_gather | solution.py:405
  257.0 116.1 %all-gather.11.cloned.1.call-start = ((), (), s32[]{:S(2)}) async-start(), calls=%async_computation.6 | async-start | bytes 5898240 | tf_op jit(solution)/shard_map/all_gather | solution.py:366
  257.6 167.7 %reduce-scatter.5.cloned.1.call-start = ((), (), s32[]{:S(2)}) async-start(), calls=%async_computation.7 | async-start | bytes 3932160 | tf_op jit(solution)/shard_map/reduce_scatter | solution.py:410
  389.0 36.2 %copy-start.1 = (bf16[192,2048]{1,0:T(8,128)(2,1)S(1)}, bf16[192,2048]{1,0:T(8,128)(2,1)}, u32[]{:S(2)}) copy-start(bf16[192,2048]{1,0:T(8,128)(2,1)} %reduce-scatter.3.cloned.1.call-done) | copy-start | bytes 2359300
Sparse Core Ops, SparseCore 0:
  9.5 108.9 all-gather.4
  130.0 38.8 reduce-scatter.2
  171.0 85.8 all-gather.6
  258.4 26.6 all-gather.8
  287.1 85.8 all-gather.10
  389.2 36.0 reduce-scatter.4
